TPU v7x, 32 devices: a whole 2x2x4 slice. The times are simulated.
32 devices in a mesh: ep: 8 (over z, x), tp: 4 (over y, core).
Axes of the slice: x: 2, y: 2, z: 4, core: 2. Of those that a mesh axis runs over, the one named last changes fastest.
Arguments:
- tokens: bfloat16 [4096, 4096], P('ep', 'tp'), may hold values from -6 to 6
- cotangent: bfloat16 [4096, 4096], P('ep', 'tp'), may hold values from -6 to 6
- expert_ids: int32 [4096, 2], P('ep'), may hold values from 0 to 15, as said below
- route_weight: float32 [4096, 2], P('ep'), may hold values from 0.1 to 1
- gate_weight: bfloat16 [16, 4096, 512], P('ep', 'tp'), may hold values from -0.09375 to 0.09375
- up_weight: bfloat16 [16, 4096, 512], P('ep', 'tp'), may hold values from -0.09375 to 0.09375
- down_weight: bfloat16 [16, 512, 4096], P('ep', None, 'tp'), may hold values from -0.25 to 0.25
- saved_gate: bfloat16 [8, 16, 128, 512], P(None, 'ep'), may hold values from -6 to 6
- saved_up: bfloat16 [8, 16, 128, 512], P(None, 'ep'), may hold values from -6 to 6
Outputs:
- token_grad: bfloat16 [4096, 4096], P('ep', 'tp')
- route_grad: float32 [4096, 2], P('ep')
- gate_weight_grad: bfloat16 [16, 4096, 512], P('ep', 'tp')
- up_weight_grad: bfloat16 [16, 4096, 512], P('ep', 'tp')
- down_weight_grad: bfloat16 [16, 512, 4096], P('ep', None, 'tp')
Inputs may be any that keep to these rules, and one draw needn't show every extreme that they name: `expert_ids`: each row names 2 different experts of one group of 4 consecutive experts. In each aligned block of 512 rows (the rows of one index of ep) no expert is named more than 128 times; the experts of one group, drawn from the seed, are named exactly 128 times in every block, and other experts may reach 128 too.
All inputs are finite; a program needn't handle non-finite values.
Results may differ from a plain program's by a relative error of at most 0.02.
Values may be sent and summed in bfloat16 or wider, within the bound.
A program may use at most 128 MiB of HBM per device.

v0:
```python
import jax
import jax.numpy as jnp
from jax import lax
from jax.sharding import PartitionSpec as P


def local(
    tokens,
    cotangent,
    expert_ids,
    route_weight,
    gate_weight,
    up_weight,
    down_weight,
    saved_gate,
    saved_up,
):
    sources = lax.axis_size("ep")
    tok_rows, width_local = tokens.shape
    top_k = expert_ids.shape[1]
    local_experts = gate_weight.shape[0]
    all_experts = local_experts * sources
    capacity = saved_gate.shape[2]
    assigned = tok_rows * top_k
    flat_ids = expert_ids.reshape(-1)
    onehot = (flat_ids[:, None] == jnp.arange(all_experts, dtype=jnp.int32)[None, :]).astype(
        jnp.int32
    )
    earlier = jnp.cumsum(onehot, axis=0) - onehot
    slot_index = jnp.sum(earlier * onehot, axis=1)
    position = flat_ids * capacity + slot_index
    slot_table = (
        jnp.full((all_experts * capacity,), assigned, jnp.int32)
        .at[position]
        .set(jnp.arange(assigned, dtype=jnp.int32))
    )
    filled = slot_table < assigned
    picked = jnp.minimum(slot_table, assigned - 1)
    token_pick = picked // top_k
    layout = (sources, local_experts, capacity, width_local)
    zero_bf = jnp.zeros((), jnp.bfloat16)
    send_tokens = jnp.where(filled[:, None], tokens[token_pick], zero_bf).reshape(layout)
    send_cot = jnp.where(filled[:, None], cotangent[token_pick], zero_bf).reshape(layout)
    send_weight = jnp.where(filled, route_weight.reshape(-1)[picked], jnp.float32(0.0)).reshape(
        layout[:3]
    )
    arrived_tokens, arrived_cot = (
        lax.all_to_all(send_tokens, "ep", split_axis=0, concat_axis=0, tiled=True),
        lax.all_to_all(send_cot, "ep", split_axis=0, concat_axis=0, tiled=True),
    )
    arrived_weight = lax.all_to_all(send_weight, "ep", split_axis=0, concat_axis=0, tiled=True)
    gate_pre = saved_gate.astype(jnp.float32)
    up_pre = saved_up.astype(jnp.float32)
    sigmoid_gate = jax.nn.sigmoid(gate_pre)
    hidden = gate_pre * sigmoid_gate * up_pre
    hidden_bf = hidden.astype(jnp.bfloat16)
    partial_back = jnp.einsum(
        "secd,efd->secf", arrived_cot, down_weight, preferred_element_type=jnp.float32
    )
    expert_out = jnp.einsum(
        "secf,efd->secd", hidden_bf, down_weight, preferred_element_type=jnp.float32
    )
    score_part = jnp.sum(expert_out * arrived_cot.astype(jnp.float32), axis=3)
    back_grad = lax.psum(partial_back.astype(jnp.bfloat16), "tp").astype(jnp.float32)
    score_total = lax.psum(score_part, "tp")
    score_back = lax.all_to_all(score_total, "ep", split_axis=0, concat_axis=0, tiled=True)
    route_grad = score_back.reshape(-1)[position].reshape(tok_rows, top_k)
    weights = arrived_weight[..., None]
    grad_hidden = weights * back_grad
    grad_up_pre = (grad_hidden * gate_pre * sigmoid_gate).astype(jnp.bfloat16)
    grad_gate_pre = (
        grad_hidden * up_pre * sigmoid_gate * (1.0 + gate_pre * (1.0 - sigmoid_gate))
    ).astype(jnp.bfloat16)
    weighted = (weights * hidden).astype(jnp.bfloat16)
    gate_weight_grad = jnp.einsum(
        "secd,secf->edf", arrived_tokens, grad_gate_pre, preferred_element_type=jnp.float32
    ).astype(jnp.bfloat16)
    up_weight_grad = jnp.einsum(
        "secd,secf->edf", arrived_tokens, grad_up_pre, preferred_element_type=jnp.float32
    ).astype(jnp.bfloat16)
    down_weight_grad = jnp.einsum(
        "secf,secd->efd", weighted, arrived_cot, preferred_element_type=jnp.float32
    ).astype(jnp.bfloat16)
    slot_grad = (
        jnp.einsum("secf,edf->secd", grad_gate_pre, gate_weight, preferred_element_type=jnp.float32)
        + jnp.einsum("secf,edf->secd", grad_up_pre, up_weight, preferred_element_type=jnp.float32)
    ).astype(jnp.bfloat16)
    grad_back = lax.all_to_all(slot_grad, "ep", split_axis=0, concat_axis=0, tiled=True)
    token_rows_back = grad_back.reshape(all_experts * capacity, width_local)[position]
    token_grad = jnp.sum(
        token_rows_back.astype(jnp.float32).reshape(tok_rows, top_k, width_local), axis=1
    ).astype(jnp.bfloat16)
    return (token_grad, route_grad, gate_weight_grad, up_weight_grad, down_weight_grad)


def solution(mesh):
    in_specs = (
        P("ep", "tp"),
        P("ep", "tp"),
        P("ep", None),
        P("ep", None),
        P("ep", "tp", None),
        P("ep", "tp", None),
        P("ep", None, "tp"),
        P(None, "ep", None, None),
        P(None, "ep", None, None),
    )
    out_specs = (
        P("ep", "tp"),
        P("ep", None),
        P("ep", "tp", None),
        P("ep", "tp", None),
        P("ep", None, "tp"),
    )
    return jax.shard_map(local, mesh=mesh, in_specs=in_specs, out_specs=out_specs, check_vma=False)
```

profile of v0, /device:TPU:0, one launch (start us, length us, event | category | flops | bytes accessed | tf_op | source)
XLA Modules:
  0.0 399.6 jit_solution(2711448094251201202)
XLA Ops:
  9.5 4.5 %reduce-window.6 = s32[16,8,128]{2,1,0:T(8,128)S(1)} reduce-window(s32[16,8,128]{2,1,0:T(8,128)S(1)} %fusion.33, s32[]{:T(128)} %constant.15.clone.1), window={size=1x1x128 pad=0_0x0_0x127_0}, to_apply=%region_0.0 | reduce-window | flops 2080768 | bytes 131076 | tf_op jit(solution)/shard_map/reduce-window
  19.9 8.6 %gather_fusion = f32[2048]{0:T(1024)S(1)} fusion(f32[1024]{0:T(1024)S(1)} %reshape.89, s32[2048]{0:T(1024)S(1)} %get-tuple-element.29), kind=kCustom, calls=%fused_computation | custom fusion | bytes 24576 | tf_op jit(solution)/shard_map/gather | solution.py:44
  29.1 7.3 %all-to-all-start = ((f32[8,2,128]{2,1,0:T(2,128)}), f32[8,2,128]{2,1,0:T(2,128)S(1)}, u32[]{:S(2)}, u32[]{:S(2)}) async-start(f32[8,2,128]{2,1,0:T(2,128)} %bitcast.4), calls=%async_computation | async-start | bytes 16384 | tf_op jit(solution)/shard_map/all_to_all | solution.py:51
  36.4 9.7 %gather_fusion.4 = bf16[2048,1024]{1,0:T(8,128)(2,1)} fusion(bf16[512,1024]{1,0:T(8,128)(2,1)S(1)} %copy-done.2, s32[2048]{0:T(1024)S(1)} %get-tuple-element.30), kind=kCustom, calls=%fused_computation.4 | custom fusion | bytes 8396800 | tf_op jit(solution)/shard_map/gather | solution.py:42
  46.1 12.4 %gather_fusion.1 = bf16[2048,1024]{1,0:T(8,128)(2,1)} fusion(bf16[512,1024]{1,0:T(8,128)(2,1)} %param.10, s32[2048]{0:T(1024)S(1)} %get-tuple-element.30), kind=kCustom, calls=%fused_computation.1 | custom fusion | bytes 8396800 | tf_op jit(solution)/shard_map/gather | solution.py:43
  58.4 5.8 %broadcast_select_fusion = (bf16[8,2,128,1024]{3,2,1,0:T(8,128)(2,1)}, bf16[8,2,128,1024]{3,2,1,0:T(8,128)(2,1)}) fusion(bf16[8,2,128,1024]{3,2,1,0:T(8,128)(2,1)} %bitcast.65, pred[8,2,128]{2,1,0:T(4,128)(4,1)S(1)} %broadcast_in_dim.38, bf16[8,2,128,1024]{3,2,1,0:T(8,128)(2,1)} %bitcast.66), kind=kLoop, calls=%fused_computation.30 | loop fusion | flops 4194304 | bytes 16779264 | tf_op jit(solution)/shard_map/jit(_where)/select_n | solution.py:42
  64.3 98.9 %all_to_all.25 = bf16[8,2,128,1024]{3,2,1,0:T(8,128)(2,1)} all-to-all(bf16[8,2,128,1024]{3,2,1,0:T(8,128)(2,1)} %get-tuple-element.32), channel_id=1, replica_groups=mesh['ep'=8,'tp'=4] {'ep'}, dimensions={0} | all-to-all | bytes 8388608 | tf_op jit(solution)/shard_map/all_to_all | solution.py:49
  163.2 4.6 %all-to-all-start.4 = ((bf16[8,2,128,1024]{3,2,1,0:T(8,128)(2,1)}), bf16[8,2,128,1024]{3,2,1,0:T(8,128)(2,1)}, u32[]{:S(2)}, u32[]{:S(2)}) async-start(bf16[8,2,128,1024]{3,2,1,0:T(8,128)(2,1)} %get-tuple-element.31), calls=%async_computation.4 | async-start | bytes 8388608 | tf_op jit(solution)/shard_map/all_to_all | solution.py:48
  167.9 6.6 %convert_bitcast_fusion = bf16[8,2,128,512]{3,2,0,1:T(8,128)(2,1)} fusion(bf16[2,512,1024]{2,1,0:T(8,128)(2,1)} %param.15, bf16[8,2,128,1024]{3,2,1,0:T(8,128)(2,1)} %all_to_all.25), kind=kOutput, calls=%fused_computation.44 | convolution fusion | flops 2148532224 | bytes 8388608 | tf_op jit(solution)/shard_map/secd,efd->secf/dot_general | solution.py:57
  174.5 7.0 %fusion = f32[8,2,128]{2,0,1:T(8,128)S(1)} fusion(bf16[8,2,128,1024]{3,2,1,0:T(8,128)(2,1)} %all_to_all.25, bf16[2,512,1024]{2,1,0:T(8,128)(2,1)} %param.15, bf16[8,2,128,512]{3,2,1,0:T(8,128)(2,1)} %param.17, bf16[8,2,128,512]{3,2,1,0:T(8,128)(2,1)} %param.16), kind=kOutput, calls=%fused_computation.7 | convolution fusion | flops 2162161664 | bytes 10493952 | tf_op jit(solution)/shard_map/secf,efd->secd/dot_general | solution.py:60
  181.5 6.9 %psum.15 = f32[8,2,128]{2,0,1:T(8,128)S(1)} all-reduce(f32[8,2,128]{2,0,1:T(8,128)S(1)} %fusion), channel_id=1, replica_groups=mesh['ep'=8,'tp'=4] {'tp'}, use_global_device_ids=true, to_apply=%region_7.8 | all-reduce | flops 2048 | bytes 16384 | tf_op jit(solution)/shard_map/psum | solution.py:65
  189.1 38.5 %all-reduce.2.cloned.1.call-done = bf16[8,2,128,512]{3,2,0,1:T(8,128)(2,1)} async-done(((bf16[8,2,128,512]{3,2,0,1:T(8,128)(2,1)}), bf16[8,2,128,512]{3,2,0,1:T(8,128)(2,1)}) %all-reduce.2.cloned.1.call-update) | async-done | bytes 2097168 | tf_op jit(solution)/shard_map/psum | solution.py:64
  227.6 5.2 %fusion.9 = (bf16[8,2,128,512]{3,2,0,1:T(8,128)(2,1)}, bf16[8,2,128,512]{3,2,0,1:T(8,128)(2,1)S(1)}) fusion(bf16[8,2,128,512]{3,2,0,1:T(8,128)(2,1)} %all-reduce.2.cloned.1.call-done, f32[8,2,128]{2,0,1:T(8,128)S(1)} %copy.81, bf16[8,2,128,512]{3,2,1,0:T(8,128)(2,1)} %param.16, bf16[8,2,128,512]{3,2,1,0:T(8,128)(2,1)} %param.17), kind=kLoop, calls=%fused_computation.23 | loop fusion | flops 17825792 | bytes 10493952 | tf_op jit(solution)/shard_map/convert_element_type | solution.py:70
  234.1 5.6 %fusion.16 = f32[2,8,128,1024]{3,2,1,0:T(8,128)} fusion(bf16[8,2,128,512]{3,2,0,1:T(8,128)(2,1)S(1)} %get-tuple-element.28, bf16[2,1024,512]{2,1,0:T(8,128)(2,1)S(1)} %copy-done), kind=kOutput, calls=%fused_computation.37 | convolution fusion | flops 2147483648 | bytes 12582912 | tf_op jit(solution)/shard_map/secf,edf->secd/dot_general | solution.py:85
  239.7 20.3 %all-to-all-done.4 = bf16[8,2,128,1024]{3,2,1,0:T(8,128)(2,1)} async-done(((bf16[8,2,128,1024]{3,2,1,0:T(8,128)(2,1)}), bf16[8,2,128,1024]{3,2,1,0:T(8,128)(2,1)}, u32[]{:S(2)}, u32[]{:S(2)}) %all-to-all-start.4) | async-done | bytes 4194336 | tf_op jit(solution)/shard_map/all_to_all | solution.py:48
  263.6 7.0 %fusion.10 = bf16[8,2,128,1024]{3,2,0,1:T(8,128)(2,1)S(1)} fusion(f32[2,8,128,1024]{3,2,1,0:T(8,128)} %fusion.16, bf16[8,2,128,512]{3,2,0,1:T(8,128)(2,1)} %get-tuple-element.27, bf16[2,1024,512]{2,1,0:T(8,128)(2,1)} %param.14), kind=kOutput, calls=%fused_computation.24 | convolution fusion | flops 2151677952 | bytes 16777216 | tf_op jit(solution)/shard_map/secf,edf->secd/dot_general | solution.py:86
  273.1 6.0 %all-to-all-start.2 = ((bf16[8,2,128,1024]{3,2,1,0:T(8,128)(2,1)}), bf16[8,2,128,1024]{3,2,1,0:T(8,128)(2,1)}, u32[]{:S(2)}, u32[]{:S(2)}) async-start(bf16[8,2,128,1024]{3,2,1,0:T(8,128)(2,1)} %copy.85), calls=%async_computation.2 | async-start | bytes 8388608 | tf_op jit(solution)/shard_map/all_to_all | solution.py:88
  279.1 7.5 %bitcast_convert_fusion = bf16[2,512,1024]{2,1,0:T(8,128)(2,1)} fusion(bf16[8,2,128,1024]{3,2,1,0:T(8,128)(2,1)} %all_to_all.25, f32[8,2,128]{2,0,1:T(8,128)S(1)} %copy.81, bf16[8,2,128,512]{3,2,1,0:T(8,128)(2,1)} %param.17, bf16[8,2,128,512]{3,2,1,0:T(8,128)(2,1)} %param.16), kind=kOutput, calls=%fused_computation.25 | convolution fusion | flops 2157969408 | bytes 10493952 | tf_op jit(solution)/shard_map/secf,secd->efd/dot_general | solution.py:81
  286.6 6.1 %gather_fusion.3 = f32[1024]{0:T(1024)S(1)} fusion(f32[2048]{0:T(1024)S(1)} %bitcast.64, s32[1024]{0:T(1024)S(1)} %broadcast_clamp_fusion), kind=kCustom, calls=%fused_computation.3 | custom fusion | bytes 12288 | tf_op jit(solution)/shard_map/gather | solution.py:67
  293.7 6.7 %bitcast_convert_fusion.1 = bf16[2,1024,512]{2,1,0:T(8,128)(2,1)} fusion(bf16[8,2,128,1024]{3,2,1,0:T(8,128)(2,1)} %all-to-all-done.4, bf16[8,2,128,512]{3,2,0,1:T(8,128)(2,1)} %get-tuple-element.27), kind=kOutput, calls=%fused_computation.26 | convolution fusion | flops 2148532224 | bytes 8388608 | tf_op jit(solution)/shard_map/secd,secf->edf/dot_general | solution.py:78
  300.4 5.9 %bitcast_convert_fusion.2 = bf16[2,1024,512]{2,1,0:T(8,128)(2,1)} fusion(bf16[8,2,128,1024]{3,2,1,0:T(8,128)(2,1)} %all-to-all-done.4, bf16[8,2,128,512]{3,2,0,1:T(8,128)(2,1)S(1)} %copy-done.4), kind=kOutput, calls=%fused_computation.27 | convolution fusion | flops 2148532224 | bytes 8388608 | tf_op jit(solution)/shard_map/secd,secf->edf/dot_general | solution.py:75
  306.2 65.8 %all-to-all-done.2 = bf16[8,2,128,1024]{3,2,1,0:T(8,128)(2,1)} async-done(((bf16[8,2,128,1024]{3,2,1,0:T(8,128)(2,1)}), bf16[8,2,128,1024]{3,2,1,0:T(8,128)(2,1)}, u32[]{:S(2)}, u32[]{:S(2)}) %all-to-all-start.2) | async-done | bytes 4194336 | tf_op jit(solution)/shard_map/all_to_all | solution.py:88
  372.0 8.9 %gather_fusion.2 = bf16[1024,1024]{1,0:T(8,128)(2,1)} fusion(bf16[2048,1024]{1,0:T(8,128)(2,1)} %bitcast.14, s32[1024]{0:T(1024)S(1)} %broadcast_clamp_fusion), kind=kCustom, calls=%fused_computation.2 | custom fusion | bytes 4198400 | tf_op jit(solution)/shard_map/gather | solution.py:89
  385.1 7.7 %reduce_sum.34 = bf16[512,1024]{1,0:T(8,128)(2,1)} reduce(bf16[512,2,1024]{2,1,0:T(2,128)(2,1)} %gather.25, bf16[]{:T(256)} %constant.36.clone.1), dimensions={1}, to_apply=%region_5.6 | reduce | flops 524288 | bytes 3145730 | tf_op jit(solution)/shard_map/reduce_sum | solution.py:90
  (44 shorter events, 21.8 us)
Async XLA Ops:
  7.2 226.9 %copy-start = (bf16[2,1024,512]{2,1,0:T(8,128)(2,1)S(1)}, bf16[2,1024,512]{2,1,0:T(8,128)(2,1)}, u32[]{:S(2)}) copy-start(bf16[2,1024,512]{2,1,0:T(8,128)(2,1)} %param.13) | copy-start | bytes 6291460
  19.9 16.5 %copy-start.2 = (bf16[512,1024]{1,0:T(8,128)(2,1)S(1)}, bf16[512,1024]{1,0:T(8,128)(2,1)}, u32[]{:S(2)}) copy-start(bf16[512,1024]{1,0:T(8,128)(2,1)} %param.9) | copy-start | bytes 3145732
  29.1 35.2 %all-to-all-start = ((f32[8,2,128]{2,1,0:T(2,128)}), f32[8,2,128]{2,1,0:T(2,128)S(1)}, u32[]{:S(2)}, u32[]{:S(2)}) async-start(f32[8,2,128]{2,1,0:T(2,128)} %bitcast.4), calls=%async_computation | async-start | bytes 16384 | tf_op jit(solution)/shard_map/all_to_all | solution.py:51
  163.2 96.8 %all-to-all-start.4 = ((bf16[8,2,128,1024]{3,2,1,0:T(8,128)(2,1)}), bf16[8,2,128,1024]{3,2,1,0:T(8,128)(2,1)}, u32[]{:S(2)}, u32[]{:S(2)}) async-start(bf16[8,2,128,1024]{3,2,1,0:T(8,128)(2,1)} %get-tuple-element.31), calls=%async_computation.4 | async-start | bytes 8388608 | tf_op jit(solution)/shard_map/all_to_all | solution.py:48
  167.8 59.7 %all-reduce.2.cloned.1.call-start = ((), (), s32[]{:S(2)}) async-start(), calls=%async_computation.5 | async-start | bytes 4194304 | tf_op jit(solution)/shard_map/psum | solution.py:64
  232.8 1.3 copy-start.3
  260.0 13.1 %all-to-all-start.3 = ((f32[8,2,128]{2,1,0:T(2,128)}), f32[8,2,128]{2,1,0:T(2,128)S(1)}, u32[]{:S(2)}, u32[]{:S(2)}) async-start(f32[8,2,128]{2,1,0:T(2,128)} %copy.87), calls=%async_computation.3 | async-start | bytes 16384 | tf_op jit(solution)/shard_map/all_to_all | solution.py:66
  273.1 98.9 %all-to-all-start.2 = ((bf16[8,2,128,1024]{3,2,1,0:T(8,128)(2,1)}), bf16[8,2,128,1024]{3,2,1,0:T(8,128)(2,1)}, u32[]{:S(2)}, u32[]{:S(2)}) async-start(bf16[8,2,128,1024]{3,2,1,0:T(8,128)(2,1)} %copy.85), calls=%async_computation.2 | async-start | bytes 8388608 | tf_op jit(solution)/shard_map/all_to_all | solution.py:88
  293.7 6.7 %copy-start.4 = (bf16[8,2,128,512]{3,2,0,1:T(8,128)(2,1)S(1)}, bf16[8,2,128,512]{3,2,0,1:T(8,128)(2,1)}, u32[]{:S(2)}) copy-start(bf16[8,2,128,512]{3,2,0,1:T(8,128)(2,1)} %copy-done.3) | copy-start | bytes 6291460
  372.0 20.7 %copy-start.1 = (bf16[2,1024,512]{2,1,0:T(8,128)(2,1)S(1)}, bf16[2,1024,512]{2,1,0:T(8,128)(2,1)}, u32[]{:S(2)}) copy-start(bf16[2,1024,512]{2,1,0:T(8,128)(2,1)} %param.13) | copy-start | bytes 6291460
Sparse Core Ops, SparseCore 0:
  174.6 52.9 all-reduce.1
where the time goes:
time: 400 us
  waiting for transfers between devices  125 us (31%)
  blocking collectives  106 us (26%)
  local copies, waits for them, and re-layouts  62.2 us (16%)
  matrix products  46.3 us (12%)
  other arithmetic  24.8 us (6%)
  starting transfers between devices  21.5 us (5%)
  between operations  14.2 us (4%)
    all_to_all x1, blocking collectives, local(): lax.all_to_all(send_cot, 'ep', split_axis=0, concat_axis=0, tiled=True)  98.9 us
    all_to_all x1, waiting for transfers between devices, local(): lax.all_to_all(slot_grad, 'ep', split_axis=0, concat_axis=0, tiled=True)  65.8 us
    psum x1, waiting for transfers between devices, local(): lax.psum(partial_back.astype(jnp.bfloat16), 'tp').astype(jnp.float32)  38.5 us
    all_to_all x1, waiting for transfers between devices, local(): lax.all_to_all(send_tokens, 'ep', split_axis=0, concat_axis=0, tiled=True)  20.3 us
    gather x2, local copies, waits for them, and re-layouts, local(): grad_back.reshape(all_experts * capacity, width_local)[position]  13 us
    gather x1, local copies, waits for them, and re-layouts, local(): cotangent[token_pick]  12.4 us
    gather x1, local copies, waits for them, and re-layouts, local(): tokens[token_pick]  9.66 us
    gather x1, local copies, waits for them, and re-layouts, local(): route_weight.reshape(-1)[picked]  8.58 us
  transfers between devices with their start and end apart: 5, of which 3 were waited for; matrix products, arithmetic and copies ran while one was open for 22% of the time, Pallas kernels for 0%

commit v1 on v0

v1 whole, which is shorter than its diff:
```python
import jax
import jax.numpy as jnp
from jax import lax
from jax.sharding import PartitionSpec as P

E_GROUP = 4
BACK_CHUNKS = 2
OUT_CHUNKS = 2
BF = jnp.bfloat16
F32 = jnp.float32


def dot32(spec, a, b):
    return jnp.einsum(spec, a, b, preferred_element_type=F32)


def sum_over_tp(part):
    if lax.axis_size("tp") != 4 or part.shape[0] % 2:
        return lax.psum(part, "tp").astype(F32)
    first = lax.axis_index("tp") % 2 == 0
    cores = [(i, i ^ 1) for i in range(4)]
    chips = [(i, i ^ 2) for i in range(4)]
    half = part.shape[0] // 2
    low, high = part[:half], part[half:]
    got = lax.ppermute(jnp.where(first, high, low), "tp", cores)
    mine = (jnp.where(first, low, high).astype(F32) + got.astype(F32)).astype(BF)
    other = lax.ppermute(mine, "tp", chips)
    mine = mine.astype(F32) + other.astype(F32)
    theirs = lax.ppermute(mine, "tp", cores)
    return jnp.concatenate(
        [jnp.where(first, mine, theirs), jnp.where(first, theirs, mine)], axis=0
    )


def local(
    tokens,
    cotangent,
    expert_ids,
    route_weight,
    gate_weight,
    up_weight,
    down_weight,
    saved_gate,
    saved_up,
):
    sources = lax.axis_size("ep")
    tok_rows, width = tokens.shape
    top_k = expert_ids.shape[1]
    local_experts = gate_weight.shape[0]
    all_experts = local_experts * sources
    capacity = saved_gate.shape[2]
    hidden_units = gate_weight.shape[2]
    span = E_GROUP // local_experts
    groups = sources // span
    group_cap = min(E_GROUP * capacity // top_k, tok_rows)
    slots = local_experts * capacity
    lane = lax.axis_index("ep") % span
    columns = [[g * span + p for g in range(groups)] for p in range(span)]

    def across(x):
        return lax.all_to_all(
            x, "ep", split_axis=0, concat_axis=0, tiled=True, axis_index_groups=columns
        )

    def shift(x, by):
        pairs = [
            (g * span + p, g * span + (p + by) % span) for g in range(groups) for p in range(span)
        ]
        return lax.ppermute(x, "ep", pairs)

    def of_lane(x, j):
        split = x.reshape((groups, span) + x.shape[1:])
        return lax.dynamic_index_in_dim(split, (lane + j) % span, axis=1, keepdims=False)

    hits = expert_ids[:, :, None] == jnp.arange(all_experts, dtype=jnp.int32)
    named = jnp.any(hits, axis=1)
    token_weight = jnp.sum(jnp.where(hits, route_weight[:, :, None], 0.0), axis=1)
    group = expert_ids[:, 0] // E_GROUP
    in_group = group[:, None] == jnp.arange(groups, dtype=jnp.int32)
    marks = jnp.concatenate([named, in_group], axis=1).astype(BF)
    ticks = jnp.arange(tok_rows, dtype=jnp.int32)
    earlier = (ticks[None, :] < ticks[:, None]).astype(BF)
    counts = dot32("ts,sm->tm", earlier, marks)
    rank = jnp.sum(jnp.where(in_group, counts[:, all_experts:], 0.0), axis=1)
    slot_key = jnp.where(named, counts[:, :all_experts], -1.0)
    place = group * group_cap + rank.astype(jnp.int32)
    pick = (
        jnp.arange(groups * group_cap, dtype=jnp.int32)[:, None] == place[None, :]
    ).astype(BF)

    def pack(x):
        return dot32("rt,td->rd", pick, x).astype(BF).reshape(groups, group_cap, x.shape[1])

    slot_hit = slot_key[:, :, None] == jnp.arange(capacity, dtype=F32)
    rank_table = jnp.sum(jnp.where(slot_hit, rank[:, None, None] + 1.0, 0.0), axis=0)
    weight_table = jnp.sum(jnp.where(slot_hit, token_weight[:, :, None], 0.0), axis=0)
    tables = jnp.stack(
        [
            rank_table.reshape(sources, slots),
            weight_table.reshape(sources, slots),
        ],
        axis=1,
    )

    step = width // BACK_CHUNKS
    cot_parts = [[] for _ in range(span)]
    token_parts = [[] for _ in range(span)]
    before = None
    for source, parts in ((cotangent, cot_parts), (tokens, token_parts)):
        for k in range(BACK_CHUNKS):
            piece = pack(source[:, k * step : (k + 1) * step])
            if before is None:
                pass
            elif len(cot_parts[0]) == 1:
                tables, before = lax.optimization_barrier((tables, before))
                tables = lax.all_to_all(tables, "ep", split_axis=0, concat_axis=0, tiled=True)
                piece, tables, before = lax.optimization_barrier((piece, tables, before))
                for (held, at), value in zip(spots, before):
                    held[at] = value
            else:
                piece, before = lax.optimization_barrier((piece, before))
                for (held, at), value in zip(spots, before):
                    held[at] = value
            parts[0].append(across(piece))
            passed_on = [(parts[j], k) for j in range(1, span)]
            for j in range(1, span):
                if source is cotangent or k + 1 < BACK_CHUNKS:
                    parts[j].append(shift(parts[0][k], -j))
            spots = [(parts[0], k)] + (last_on if before is not None else [])
            before = [held[at] for held, at in spots]
            last_on = passed_on

    both_weight = jnp.concatenate([gate_weight, up_weight], axis=2)

    spread, weights, cot_slots, partial = [], [], [], []
    for j in range(span):
        table = of_lane(tables, j)
        spread.append(
            (table[:, 0, :, None] - 1.0 == jnp.arange(group_cap, dtype=F32)).astype(BF)
        )
        weights.append(table[:, 1].reshape(groups, local_experts, capacity, 1))
        cot_rows = jnp.concatenate(cot_parts[j], axis=2)
        rows = dot32("gst,gtd->gsd", spread[j], cot_rows).astype(BF)
        cot_slots.append(rows.reshape(groups, local_experts, capacity, width))
        partial.append(dot32("gecd,efd->gecf", cot_slots[j], down_weight).astype(BF))

    summed = [sum_over_tp(part) for part in partial]

    both_grad, weighted, scores = [], [], []
    for j in range(span):
        gate_pre = of_lane(saved_gate, j).astype(F32)
        up_pre = of_lane(saved_up, j).astype(F32)
        back = summed[j]
        sigmoid_gate = jax.nn.sigmoid(gate_pre)
        hidden = gate_pre * sigmoid_gate * up_pre
        scores.append(jnp.sum(hidden.astype(BF).astype(F32) * back, axis=3))
        grad_hidden = weights[j] * back
        grad_up = (grad_hidden * gate_pre * sigmoid_gate).astype(BF)
        grad_gate = (
            grad_hidden * up_pre * sigmoid_gate * (1.0 + gate_pre * (1.0 - sigmoid_gate))
        ).astype(BF)
        both_grad.append(jnp.concatenate([grad_gate, grad_up], axis=3))
        weighted.append((weights[j] * hidden).astype(BF))

    both_grad, token_parts = lax.optimization_barrier((both_grad, token_parts))

    score_lanes = jnp.stack(scores, axis=1)
    score_send = jnp.stack(
        [
            lax.dynamic_index_in_dim(score_lanes, (q - lane) % span, axis=1, keepdims=False)
            for q in range(span)
        ],
        axis=1,
    ).reshape(sources, local_experts, capacity)

    step = width // OUT_CHUNKS

    def rows_of(j, k):
        weight_k = both_weight[:, k * step : (k + 1) * step]
        grad = dot32("gecf,edf->gecd", both_grad[j], weight_k).astype(BF)
        return dot32("gst,gsd->gtd", spread[j], grad.reshape(groups, slots, step))

    sends = [[rows_of(j, k).astype(BF) for j in range(1, span)] for k in range(OUT_CHUNKS)]
    sends[0], score_send = lax.optimization_barrier((sends[0], score_send))
    ahead = lax.all_to_all(score_send, "ep", split_axis=0, concat_axis=0, tiled=True)
    out_parts = []
    for k in range(OUT_CHUNKS):
        others = [shift(x, j + 1) for j, x in enumerate(sends[k])]
        total = rows_of(0, k)
        if k + 1 == OUT_CHUNKS:
            late, others = lax.optimization_barrier((token_parts[0][-1], others))
            token_parts[0][-1] = late
            for j in range(1, span):
                token_parts[j].append(shift(late, -j))
        for other in others:
            total = total + other.astype(F32)
        total = total.astype(BF)
        if k == 0:
            total, score_back = lax.optimization_barrier((total, ahead))
        if k + 1 < OUT_CHUNKS:
            total, sends[k + 1] = lax.optimization_barrier((total, sends[k + 1]))
        out_parts.append(across(total))
    token_grad = jnp.concatenate(
        [
            dot32("rt,rd->td", pick, part.reshape(groups * group_cap, step)).astype(BF)
            for part in out_parts
        ],
        axis=1,
    )

    score_table = score_back.reshape(all_experts, capacity)
    choice_hits = hits.reshape(-1, all_experts)
    choice_slot = jnp.sum(jnp.where(hits, counts[:, None, :all_experts], 0.0), axis=2)
    choice_rows = jnp.dot(
        choice_hits.astype(F32), score_table, precision=lax.Precision.HIGHEST
    )
    choice_slot_hit = choice_slot.reshape(-1, 1) == jnp.arange(capacity, dtype=F32)
    route_grad = jnp.sum(jnp.where(choice_slot_hit, choice_rows, 0.0), axis=1)
    route_grad = route_grad.reshape(tok_rows, top_k)

    all_tokens = jnp.concatenate(
        [
            dot32("gst,gtd->gsd", spread[j], jnp.concatenate(token_parts[j], axis=2))
            .astype(BF)
            .reshape(groups, local_experts, capacity, width)
            for j in range(span)
        ],
        axis=0,
    )
    all_cot = jnp.concatenate(cot_slots, axis=0)
    all_both = jnp.concatenate(both_grad, axis=0)
    all_weighted = jnp.concatenate(weighted, axis=0)
    gate_weight_grad = dot32("secd,secf->edf", all_tokens, all_both[..., :hidden_units]).astype(BF)
    up_weight_grad = dot32("secd,secf->edf", all_tokens, all_both[..., hidden_units:]).astype(BF)
    down_weight_grad = dot32("secf,secd->efd", all_weighted, all_cot).astype(BF)
    return (token_grad, route_grad, gate_weight_grad, up_weight_grad, down_weight_grad)


def solution(mesh):
    in_specs = (
        P("ep", "tp"),
        P("ep", "tp"),
        P("ep", None),
        P("ep", None),
        P("ep", "tp", None),
        P("ep", "tp", None),
        P("ep", None, "tp"),
        P(None, "ep", None, None),
        P(None, "ep", None, None),
    )
    out_specs = (
        P("ep", "tp"),
        P("ep", None),
        P("ep", "tp", None),
        P("ep", "tp", None),
        P("ep", None, "tp"),
    )
    return jax.shard_map(local, mesh=mesh, in_specs=in_specs, out_specs=out_specs, check_vma=False)
```

time: 400 us -> 255 us (0.64)
  blocking collectives: 106 us -> 0 us
  local copies, waits for them, and re-layouts: 62.2 us -> 27.2 us
  waiting for transfers between devices: 125 us -> 97.6 us
  starting transfers between devices: 21.5 us -> 43.2 us
  matrix products: 46.3 us -> 60.1 us
  between operations: 14.2 us -> 1.25 us
    all_to_all x1 -> x0, blocking collectives: 98.9 us -> none  [local(): lax.all_to_all(send_cot, 'ep', split_axis=0, concat_axis=0, tiled=True)]
    ppermute x0 -> x12, waiting for transfers between devices: none -> 71.7 us  [the longest x6 70.2 us: shift(): return lax.ppermute(x, 'ep', pairs)]
    all_to_all x4 -> x8, waiting for transfers between devices: 86.1 us -> 25.9 us  [the longest x6 22.1 us: across(): lax.all_to_all(x, 'ep', split_axis=0, concat_axis=0, tiled=True, axis_ind...]
    gather x6 -> x0, local copies, waits for them, and re-layouts: 49.8 us -> none  [the longest x2 13 us: local(): grad_back.reshape(all_experts * capacity, width_local)[position]]
    psum x1 -> x0, waiting for transfers between devices: 38.5 us -> none  [local(): lax.psum(partial_back.astype(jnp.bfloat16), 'tp').astype(jnp.float32)]
    all_to_all x4 -> x8, starting transfers between devices: 21.5 us -> 36 us  [the longest x6 27.6 us: across(): lax.all_to_all(x, 'ep', split_axis=0, concat_axis=0, tiled=True, axis_ind...]
    dot_general x7 -> x25, matrix products: 46.3 us -> 60.1 us  [the longest x24 59.5 us: dot32(): return jnp.einsum(spec, a, b, preferred_element_type=F32)]
    unnamed x13 -> x69, local copies, waits for them, and re-layouts: 3.71 us -> 13.2 us
  transfers between devices with their start and end apart: 5 -> 20, of which waited for: 3 -> 13; matrix products, arithmetic and copies ran while one was open for 22% -> 35% of each run, Pallas kernels for 0% -> 0%
where the time goes in v1:
time: 255 us; the launch traced here: 253 us
  waiting for transfers between devices  97.6 us (38%)
  matrix products  60.1 us (24%)
  starting transfers between devices  43.2 us (17%)
  local copies, waits for them, and re-layouts  27.2 us (11%)
  other arithmetic  23.5 us (9%)
    ppermute x6, waiting for transfers between devices, shift(): return lax.ppermute(x, 'ep', pairs)  70.2 us
    dot_general x24, matrix products, dot32(): return jnp.einsum(spec, a, b, preferred_element_type=F32)  59.5 us
    all_to_all x6, starting transfers between devices, across(): lax.all_to_all(x, 'ep', split_axis=0, concat_axis=0, tiled=True, axis_ind...  27.6 us
    all_to_all x6, waiting for transfers between devices, across(): lax.all_to_all(x, 'ep', split_axis=0, concat_axis=0, tiled=True, axis_ind...  22.1 us
    unnamed x69, local copies, waits for them, and re-layouts  13.2 us
    reshape x2, local copies, waits for them, and re-layouts, local(): all_tokens = jnp.concatenate([dot32('gst,gtd->gsd', spread[j], jnp.concat...  8.19 us
    reduce_sum x1, other arithmetic, local(): jnp.sum(jnp.where(slot_hit, rank[:, None, None] + 1.0, 0.0), axis=0)  5.12 us
  transfers between devices with their start and end apart: 20, of which 13 were waited for; matrix products, arithmetic and copies ran while one was open for 35% of the time, Pallas kernels for 0%

profile of v1, /device:TPU:0, one launch (start us, length us, event | category | flops | bytes accessed | tf_op | source)
XLA Modules:
  0.0 252.8 jit_solution(7918888312755637353)
XLA Ops:
  5.3 6.3 %all-to-all-start = ((bf16[4,256,512]{2,1,0:T(8,128)(2,1)}), bf16[4,256,512]{2,1,0:T(8,128)(2,1)S(1)}, u32[]{:S(2)}, u32[]{:S(2)}) async-start(bf16[4,256,512]{2,1,0:T(8,128)(2,1)} %bitcast.175), calls=%async_computation | async-start | bytes 2097152 | tf_op jit(solution)/shard_map/all_to_all | solution.py:61
  12.7 5.1 %select_reduce_fusion.1 = (f32[16,128]{1,0:T(8,128)S(1)}, f32[16,128]{1,0:T(8,128)S(1)}) fusion(f32[512]{0:T(512)S(1)} %broadcast_add_fusion, f32[512,16]{1,0:T(8,128)} %copy.141, f32[512,16]{1,0:T(8,128)S(1)} %copy.142), kind=kLoop, calls=%fused_computation.8 | loop fusion | flops 5238784 | bytes 83968 | tf_op jit(solution)/shard_map/reduce_sum | solution.py:95
  18.4 18.9 %all-to-all-done = bf16[4,256,512]{2,1,0:T(8,128)(2,1)S(1)} async-done(((bf16[4,256,512]{2,1,0:T(8,128)(2,1)}), bf16[4,256,512]{2,1,0:T(8,128)(2,1)S(1)}, u32[]{:S(2)}, u32[]{:S(2)}) %all-to-all-start) | async-done | bytes 1048608 | tf_op jit(solution)/shard_map/all_to_all | solution.py:61
  37.3 3.7 %all-to-all-start.1 = ((f32[8,2,256]{2,1,0:T(2,128)}), f32[8,2,256]{2,1,0:T(2,128)S(1)}, u32[]{:S(2)}, u32[]{:S(2)}) async-start(f32[8,2,256]{2,1,0:T(2,128)} %pad_maximum_fusion.13), calls=%async_computation.1 | async-start | bytes 32768 | tf_op jit(solution)/shard_map/all_to_all | solution.py:116
  43.7 3.8 %all-to-all-done.1 = f32[8,2,256]{2,1,0:T(2,128)S(1)} async-done(((f32[8,2,256]{2,1,0:T(2,128)}), f32[8,2,256]{2,1,0:T(2,128)S(1)}, u32[]{:S(2)}, u32[]{:S(2)}) %all-to-all-start.1) | async-done | bytes 16416 | tf_op jit(solution)/shard_map/all_to_all | solution.py:116
  47.6 4.3 %all-to-all-start.2 = ((bf16[4,256,512]{2,1,0:T(8,128)(2,1)}), bf16[4,256,512]{2,1,0:T(8,128)(2,1)}, u32[]{:S(2)}, u32[]{:S(2)}) async-start(bf16[4,256,512]{2,1,0:T(8,128)(2,1)} %bitcast.173), calls=%async_computation.2 | async-start | bytes 2097152 | tf_op jit(solution)/shard_map/all_to_all | solution.py:61
  55.2 19.5 %collective-permute-done = bf16[4,256,512]{2,1,0:T(8,128)(2,1)} collective-permute-done((bf16[4,256,512]{2,1,0:T(8,128)(2,1)S(1)}, bf16[4,256,512]{2,1,0:T(8,128)(2,1)}, u32[]{:S(2)}, u32[]{:S(2)}) %collective-permute-start) | collective-permute-done | bytes 1048608 | tf_op jit(solution)/shard_map/ppermute | solution.py:69
  75.7 4.3 %all-to-all-start.3 = ((bf16[4,256,512]{2,1,0:T(8,128)(2,1)}), bf16[4,256,512]{2,1,0:T(8,128)(2,1)}, u32[]{:S(2)}, u32[]{:S(2)}) async-start(bf16[4,256,512]{2,1,0:T(8,128)(2,1)} %bitcast.174), calls=%async_computation.3 | async-start | bytes 2097152 | tf_op jit(solution)/shard_map/all_to_all | solution.py:61
  87.8 18.7 %collective-permute-done.4 = bf16[4,256,512]{2,1,0:T(8,128)(2,1)} collective-permute-done((bf16[4,256,512]{2,1,0:T(8,128)(2,1)}, bf16[4,256,512]{2,1,0:T(8,128)(2,1)}, u32[]{:S(2)}, u32[]{:S(2)}) %collective-permute-start.4) | collective-permute-done | bytes 1048608 | tf_op jit(solution)/shard_map/ppermute | solution.py:69
  122.0 4.8 %all-to-all-start.4 = ((bf16[4,256,512]{2,1,0:T(8,128)(2,1)}), bf16[4,256,512]{2,1,0:T(8,128)(2,1)}, u32[]{:S(2)}, u32[]{:S(2)}) async-start(bf16[4,256,512]{2,1,0:T(8,128)(2,1)} %bitcast.172), calls=%async_computation.4 | async-start | bytes 2097152 | tf_op jit(solution)/shard_map/all_to_all | solution.py:61
  140.0 11.8 %collective-permute-done.8 = bf16[4,256,512]{2,1,0:T(8,128)(2,1)} collective-permute-done((bf16[4,256,512]{2,1,0:T(8,128)(2,1)}, bf16[4,256,512]{2,1,0:T(8,128)(2,1)}, u32[]{:S(2)}, u32[]{:S(2)}) %collective-permute-start.8) | collective-permute-done | bytes 1048608 | tf_op jit(solution)/shard_map/ppermute | solution.py:69
  152.6 3.5 %fusion.107 = bf16[4,2,128,512]{3,2,0,1:T(8,128)(2,1)S(1)} fusion(bf16[4,2,128,1024]{3,2,0,1:T(8,128)(2,1)} %pad_maximum_fusion.7, bf16[2,1024,1024]{2,1,0:T(8,128)(2,1)} %copy-done.19), kind=kOutput, calls=%fused_computation.110 | convolution fusion | flops 1074266112 | bytes 5242880 | tf_op jit(solution)/shard_map/gecf,edf->gecd/dot_general | solution.py:14
  164.5 4.7 %all-to-all-start.5 = ((f32[8,2,128]{2,1,0:T(2,128)}), f32[8,2,128]{2,1,0:T(2,128)S(1)}, u32[]{:S(2)}, u32[]{:S(2)}) async-start(f32[8,2,128]{2,1,0:T(2,128)} %copy.157), calls=%async_computation.5 | async-start | bytes 16384 | tf_op jit(solution)/shard_map/all_to_all | solution.py:185
  172.1 10.5 %collective-permute-done.9 = bf16[4,256,512]{2,1,0:T(8,128)(2,1)} collective-permute-done((bf16[4,256,512]{2,1,0:T(8,128)(2,1)}, bf16[4,256,512]{2,1,0:T(8,128)(2,1)}, u32[]{:S(2)}, u32[]{:S(2)}) %collective-permute-start.9) | collective-permute-done | bytes 1048608 | tf_op jit(solution)/shard_map/ppermute | solution.py:69
  189.0 4.5 %all-to-all-start.6 = ((bf16[4,256,512]{2,1,0:T(8,128)(2,1)}), bf16[4,256,512]{2,1,0:T(8,128)(2,1)}, u32[]{:S(2)}, u32[]{:S(2)}) async-start(bf16[4,256,512]{2,1,0:T(8,128)(2,1)} %add_convert_fusion.1), calls=%async_computation.6 | async-start | bytes 2097152 | tf_op jit(solution)/shard_map/all_to_all | solution.py:61
  197.7 3.6 %bitcast_convert_fusion = bf16[2,512,1024]{2,1,0:T(8,128)(2,1)} fusion(bf16[4,2,128,512]{3,2,0,1:T(8,128)(2,1)S(1)} %copy-done.22, bf16[4,2,128,512]{3,2,0,1:T(8,128)(2,1)S(1)} %copy-done.21, bf16[4,2,128,1024]{3,2,1,0:T(8,128)(2,1)S(1)} %bitcast.200, bf16[4,2,128,1024]{3,2,1,0:T(8,128)(2,1)S(1)} %bitcast.198), kind=kOutput, calls=%fused_computation.2 | convolution fusion | flops 2151677952 | bytes 8388608 | tf_op jit(solution)/shard_map/secf,secd->efd/dot_general | solution.py:14
  201.3 7.8 %collective-permute-done.10 = bf16[4,256,512]{2,1,0:T(8,128)(2,1)} collective-permute-done((bf16[4,256,512]{2,1,0:T(8,128)(2,1)}, bf16[4,256,512]{2,1,0:T(8,128)(2,1)}, u32[]{:S(2)}, u32[]{:S(2)}) %collective-permute-start.10) | collective-permute-done | bytes 1048608 | tf_op jit(solution)/shard_map/ppermute | solution.py:69
  213.4 3.6 %fusion.58 = bf16[4,256,1024]{2,1,0:T(8,128)(2,1)} fusion(bf16[4,256,512]{2,1,0:T(8,128)(2,1)} %all-to-all-done.4, bf16[4,256,512]{2,1,0:T(8,128)(2,1)} %all-to-all-done.3, f32[4,256]{1,0:T(4,128)S(1)} %bitcast.181), kind=kOutput, calls=%fused_computation.89 | convolution fusion | flops 542375936 | bytes 4198400 | tf_op jit(solution)/shard_map/gst,gtd->gsd/dot_general | solution.py:14
  217.0 4.1 %copy.164 = bf16[4,2,128,1024]{2,3,0,1:T(8,128)(2,1)} copy(bf16[4,2,128,1024]{3,2,1,0:T(8,128)(2,1)} %bitcast.171) | data formatting | bytes 4194304 | tf_op jit(solution)/shard_map/reshape | solution.py:225
  223.6 3.5 %all-to-all-start.7 = ((bf16[4,256,512]{2,1,0:T(8,128)(2,1)}), bf16[4,256,512]{2,1,0:T(8,128)(2,1)S(1)}, u32[]{:S(2)}, u32[]{:S(2)}) async-start(bf16[4,256,512]{2,1,0:T(8,128)(2,1)} %add_convert_fusion), calls=%async_computation.7 | async-start | bytes 2097152 | tf_op jit(solution)/shard_map/all_to_all | solution.py:61
  231.9 3.6 %fusion.55 = bf16[4,256,1024]{2,1,0:T(8,128)(2,1)} fusion(bf16[4,256,512]{2,1,0:T(8,128)(2,1)} %collective-permute-done.11, bf16[4,256,512]{2,1,0:T(8,128)(2,1)} %collective-permute-done.8, f32[4,256]{1,0:T(4,128)S(1)} %bitcast.185), kind=kOutput, calls=%fused_computation.88 | convolution fusion | flops 542375936 | bytes 4198400 | tf_op jit(solution)/shard_map/gst,gtd->gsd/dot_general | solution.py:14
  235.5 4.1 %copy.165 = bf16[4,2,128,1024]{2,3,0,1:T(8,128)(2,1)} copy(bf16[4,2,128,1024]{3,2,1,0:T(8,128)(2,1)} %bitcast.170) | data formatting | bytes 4194304 | tf_op jit(solution)/shard_map/reshape | solution.py:225
  239.6 6.0 %bitcast_convert_fusion.1 = bf16[2,1024,512]{2,1,0:T(8,128)(2,1)} fusion(bf16[8,2,128,1024]{3,2,0,1:T(8,128)(2,1)} %copy-done.17, bf16[4,2,128,1024]{2,3,0,1:T(8,128)(2,1)} %copy.165, bf16[4,2,128,1024]{2,3,0,1:T(8,128)(2,1)S(1)} %copy-done.13), kind=kOutput, calls=%fused_computation.5 | convolution fusion | flops 2150629376 | bytes 8388608 | tf_op jit(solution)/shard_map/secd,secf->edf/dot_general | solution.py:14
  245.6 3.5 %bitcast_convert_fusion.2 = bf16[2,1024,512]{2,1,0:T(8,128)(2,1)} fusion(bf16[8,2,128,1024]{3,2,0,1:T(8,128)(2,1)S(1)} %copy-done.18, bf16[4,2,128,1024]{2,3,0,1:T(8,128)(2,1)S(1)} %copy-done.14, bf16[4,2,128,1024]{2,3,0,1:T(8,128)(2,1)S(1)} %copy-done.13), kind=kOutput, calls=%fused_computation.6 | convolution fusion | flops 2150629376 | bytes 8388608 | tf_op jit(solution)/shard_map/secd,secf->edf/dot_general | solution.py:14
  (156 shorter events, 87.4 us)
Async XLA Ops:
  0.6 81.9 %copy-start = (bf16[2,512,1024]{2,1,0:T(8,128)(2,1)S(1)}, bf16[2,512,1024]{2,1,0:T(8,128)(2,1)}, u32[]{:S(2)}) copy-start(bf16[2,512,1024]{2,1,0:T(8,128)(2,1)} %param.15) | copy-start | bytes 6291460
  2.5 9.1 %copy-start.24 = (s32[512,2]{0,1:T(2,128)S(1)}, s32[512,2]{0,1:T(2,128)}, u32[]{:S(2)}) copy-start(s32[512,2]{0,1:T(2,128)} %param.11) | copy-start | bytes 12292
  2.5 9.1 %copy-start.25 = (f32[512,2]{0,1:T(2,128)S(1)}, f32[512,2]{0,1:T(2,128)}, u32[]{:S(2)}) copy-start(f32[512,2]{0,1:T(2,128)} %param.12) | copy-start | bytes 12292
  5.3 32.1 %all-to-all-start = ((bf16[4,256,512]{2,1,0:T(8,128)(2,1)}), bf16[4,256,512]{2,1,0:T(8,128)(2,1)S(1)}, u32[]{:S(2)}, u32[]{:S(2)}) async-start(bf16[4,256,512]{2,1,0:T(8,128)(2,1)} %bitcast.175), calls=%async_computation | async-start | bytes 2097152 | tf_op jit(solution)/shard_map/all_to_all | solution.py:61
  37.3 10.2 %all-to-all-start.1 = ((f32[8,2,256]{2,1,0:T(2,128)}), f32[8,2,256]{2,1,0:T(2,128)S(1)}, u32[]{:S(2)}, u32[]{:S(2)}) async-start(f32[8,2,256]{2,1,0:T(2,128)} %pad_maximum_fusion.13), calls=%async_computation.1 | async-start | bytes 32768 | tf_op jit(solution)/shard_map/all_to_all | solution.py:116
  47.6 28.1 %all-to-all-start.2 = ((bf16[4,256,512]{2,1,0:T(8,128)(2,1)}), bf16[4,256,512]{2,1,0:T(8,128)(2,1)}, u32[]{:S(2)}, u32[]{:S(2)}) async-start(bf16[4,256,512]{2,1,0:T(8,128)(2,1)} %bitcast.173), calls=%async_computation.2 | async-start | bytes 2097152 | tf_op jit(solution)/shard_map/all_to_all | solution.py:61
  51.9 22.8 %collective-permute-start = (bf16[4,256,512]{2,1,0:T(8,128)(2,1)S(1)}, bf16[4,256,512]{2,1,0:T(8,128)(2,1)}, u32[]{:S(2)}, u32[]{:S(2)}) collective-permute-start(bf16[4,256,512]{2,1,0:T(8,128)(2,1)S(1)} %all-to-all-done), channel_id=1, source_target_pairs={{0,4},{4,0},{8,12},{12,8},{16,20},{20,16},{24,28},{28,24},{1,5},{5... | collective-permute-start | bytes 3145736 | tf_op jit(solution)/shard_map/ppermute | solution.py:69
  75.7 30.8 %all-to-all-start.3 = ((bf16[4,256,512]{2,1,0:T(8,128)(2,1)}), bf16[4,256,512]{2,1,0:T(8,128)(2,1)}, u32[]{:S(2)}, u32[]{:S(2)}) async-start(bf16[4,256,512]{2,1,0:T(8,128)(2,1)} %bitcast.174), calls=%async_computation.3 | async-start | bytes 2097152 | tf_op jit(solution)/shard_map/all_to_all | solution.py:61
  81.9 24.6 %collective-permute-start.4 = (bf16[4,256,512]{2,1,0:T(8,128)(2,1)}, bf16[4,256,512]{2,1,0:T(8,128)(2,1)}, u32[]{:S(2)}, u32[]{:S(2)}) collective-permute-start(bf16[4,256,512]{2,1,0:T(8,128)(2,1)} %all-to-all-done.2), channel_id=1, source_target_pairs={{0,4},{4,0},{8,12},{12,8},{16,20},{20,16},{24,28},{28,24},{1,5},{5... | collective-permute-start | bytes 3145736 | tf_op jit(solution)/shard_map/ppermute | solution.py:69
  84.0 2.0 collective-permute-start.1
  86.2 26.5 %collective-permute-start.2 = (bf16[2,2,128,512]{3,2,0,1:T(8,128)(2,1)S(1)}, bf16[2,2,128,512]{3,2,0,1:T(8,128)(2,1)S(1)}, u32[]{:S(2)}, u32[]{:S(2)}) collective-permute-start(bf16[2,2,128,512]{3,2,0,1:T(8,128)(2,1)S(1)} %add_convert_fusion.3), channel_id=1, source_target_pairs={{0,2},{1,3},{2,0},{3,1},{4,6},{5,7},{6,4},{7,5},{8,10},{9,11},{10,... | collective-permute-start | bytes 1572872 | tf_op jit(solution)/shard_map/ppermute | solution.py:27
  112.0 2.3 collective-permute-start.5
  113.9 16.0 %collective-permute-start.3 = (f32[2,2,128,512]{3,2,0,1:T(8,128)}, f32[2,2,128,512]{3,2,0,1:T(8,128)}, u32[]{:S(2)}, u32[]{:S(2)}) collective-permute-start(f32[2,2,128,512]{3,2,0,1:T(8,128)} %convert_add_fusion.1), channel_id=1, source_target_pairs={{0,1},{1,0},{2,3},{3,2},{4,5},{5,4},{6,7},{7,6},{8,9},{9,8},{10,11... | collective-permute-start | bytes 3145736 | tf_op jit(solution)/shard_map/ppermute | solution.py:29
  114.6 14.0 %collective-permute-start.6 = (bf16[2,2,128,512]{3,2,0,1:T(8,128)(2,1)S(1)}, bf16[2,2,128,512]{3,2,0,1:T(8,128)(2,1)}, u32[]{:S(2)}, u32[]{:S(2)}) collective-permute-start(bf16[2,2,128,512]{3,2,0,1:T(8,128)(2,1)S(1)} %add_convert_fusion.2), channel_id=1, source_target_pairs={{0,2},{1,3},{2,0},{3,1},{4,6},{5,7},{6,4},{7,5},{8,10},{9,11},{10,... | collective-permute-start | bytes 1572872 | tf_op jit(solution)/shard_map/ppermute | solution.py:27
  122.0 30.6 %all-to-all-start.4 = ((bf16[4,256,512]{2,1,0:T(8,128)(2,1)}), bf16[4,256,512]{2,1,0:T(8,128)(2,1)}, u32[]{:S(2)}, u32[]{:S(2)}) async-start(bf16[4,256,512]{2,1,0:T(8,128)(2,1)} %bitcast.172), calls=%async_computation.4 | async-start | bytes 2097152 | tf_op jit(solution)/shard_map/all_to_all | solution.py:61
  126.8 25.0 %collective-permute-start.8 = (bf16[4,256,512]{2,1,0:T(8,128)(2,1)}, bf16[4,256,512]{2,1,0:T(8,128)(2,1)}, u32[]{:S(2)}, u32[]{:S(2)}) collective-permute-start(bf16[4,256,512]{2,1,0:T(8,128)(2,1)} %all-to-all-done.3), channel_id=1, source_target_pairs={{0,4},{4,0},{8,12},{12,8},{16,20},{20,16},{24,28},{28,24},{1,5},{5... | collective-permute-start | bytes 3145736 | tf_op jit(solution)/shard_map/ppermute | solution.py:69
  129.8 4.4 %collective-permute-start.7 = (f32[2,2,128,512]{3,2,0,1:T(8,128)S(1)}, f32[2,2,128,512]{3,2,0,1:T(8,128)S(1)}, u32[]{:S(2)}, u32[]{:S(2)}) collective-permute-start(f32[2,2,128,512]{3,2,0,1:T(8,128)S(1)} %convert_add_fusion), channel_id=1, source_target_pairs={{0,1},{1,0},{2,3},{3,2},{4,5},{5,4},{6,7},{7,6},{8,9},{9,8},{10,11... | collective-permute-start | bytes 3145736 | tf_op jit(solution)/shard_map/ppermute | solution.py:29
  157.9 24.6 %collective-permute-start.9 = (bf16[4,256,512]{2,1,0:T(8,128)(2,1)}, bf16[4,256,512]{2,1,0:T(8,128)(2,1)}, u32[]{:S(2)}, u32[]{:S(2)}) collective-permute-start(bf16[4,256,512]{2,1,0:T(8,128)(2,1)} %convolution_convert_fusion.1), channel_id=1, source_target_pairs={{0,4},{4,0},{8,12},{12,8},{16,20},{20,16},{24,28},{28,24},{1,5},{5... | collective-permute-start | bytes 3145736 | tf_op jit(solution)/shard_map/ppermute | solution.py:69
  164.5 21.0 %all-to-all-start.5 = ((f32[8,2,128]{2,1,0:T(2,128)}), f32[8,2,128]{2,1,0:T(2,128)S(1)}, u32[]{:S(2)}, u32[]{:S(2)}) async-start(f32[8,2,128]{2,1,0:T(2,128)} %copy.157), calls=%async_computation.5 | async-start | bytes 16384 | tf_op jit(solution)/shard_map/all_to_all | solution.py:185
  185.5 23.6 %collective-permute-start.10 = (bf16[4,256,512]{2,1,0:T(8,128)(2,1)}, bf16[4,256,512]{2,1,0:T(8,128)(2,1)}, u32[]{:S(2)}, u32[]{:S(2)}) collective-permute-start(bf16[4,256,512]{2,1,0:T(8,128)(2,1)} %convolution_convert_fusion), channel_id=1, source_target_pairs={{0,4},{4,0},{8,12},{12,8},{16,20},{20,16},{24,28},{28,24},{1,5},{5... | collective-permute-start | bytes 3145736 | tf_op jit(solution)/shard_map/ppermute | solution.py:69
  189.0 34.7 %all-to-all-start.6 = ((bf16[4,256,512]{2,1,0:T(8,128)(2,1)}), bf16[4,256,512]{2,1,0:T(8,128)(2,1)}, u32[]{:S(2)}, u32[]{:S(2)}) async-start(bf16[4,256,512]{2,1,0:T(8,128)(2,1)} %add_convert_fusion.1), calls=%async_computation.6 | async-start | bytes 2097152 | tf_op jit(solution)/shard_map/all_to_all | solution.py:61
  197.7 11.9 %copy-start.3 = (bf16[4,2,128,1024]{3,2,0,1:T(8,128)(2,1)S(1)}, bf16[4,2,128,1024]{3,2,0,1:T(8,128)(2,1)}, u32[]{:S(2)}) copy-start(bf16[4,2,128,1024]{3,2,0,1:T(8,128)(2,1)} %pad_maximum_fusion.7) | copy-start | bytes 6291460
  209.1 22.8 %collective-permute-start.11 = (bf16[4,256,512]{2,1,0:T(8,128)(2,1)}, bf16[4,256,512]{2,1,0:T(8,128)(2,1)}, u32[]{:S(2)}, u32[]{:S(2)}) collective-permute-start(bf16[4,256,512]{2,1,0:T(8,128)(2,1)} %all-to-all-done.4), channel_id=1, source_target_pairs={{0,4},{4,0},{8,12},{12,8},{16,20},{20,16},{24,28},{28,24},{1,5},{5... | collective-permute-start | bytes 3145736 | tf_op jit(solution)/shard_map/ppermute | solution.py:69
  223.6 26.8 %all-to-all-start.7 = ((bf16[4,256,512]{2,1,0:T(8,128)(2,1)}), bf16[4,256,512]{2,1,0:T(8,128)(2,1)S(1)}, u32[]{:S(2)}, u32[]{:S(2)}) async-start(bf16[4,256,512]{2,1,0:T(8,128)(2,1)} %add_convert_fusion), calls=%async_computation.7 | async-start | bytes 2097152 | tf_op jit(solution)/shard_map/all_to_all | solution.py:61
  (27 other events, 67.1 us)
